TPU v7x, 32 devices: a whole 2x2x4 slice. The times are simulated.
32 devices in a mesh: ep: 8 (over z, x), tp: 4 (over y, core).
Axes of the slice: x: 2, y: 2, z: 4, core: 2. Of those that a mesh axis runs over, the one named last changes fastest.
Arguments:
- tokens: bfloat16 [1024, 2048], P('ep', 'tp'), may hold values from -20 to 20
- routing: int32 [1024, 2], P('ep'), may hold values from 0 to 7, all different within a row; in each aligned block of 128 rows (0 to 127, 128 to 255, ...) at most 48 rows name the same one
- gate_weights: bfloat16 [1024, 2], P('ep'), may hold values from 0 to 1, as said below
- cotangent: bfloat16 [1024, 2048], P('ep', 'tp'), may hold values from -3 to 3
- expert_gate: bfloat16 [8, 2048, 3072], P('ep', None, 'tp'), may hold values from -3 to 3
- expert_up: bfloat16 [8, 2048, 3072], P('ep', None, 'tp'), may hold values from -3 to 3
- expert_down: bfloat16 [8, 3072, 2048], P('ep', 'tp'), may hold values from -0.109375 to 0.109375
- router: bfloat16 [2048, 8], replicated, may hold values from -0.125 to 0.125
Outputs:
- token_grad: float32 [1024, 2048], P('ep', 'tp')
- gate_grad: float32 [1024, 2], P('ep')
- gate_proj_grad: bfloat16 [8, 2048, 3072], P('ep', None, 'tp')
- up_proj_grad: bfloat16 [8, 2048, 3072], P('ep', None, 'tp')
- down_proj_grad: bfloat16 [8, 3072, 2048], P('ep', 'tp')
- router_grad: float32 [8, 2048], P('ep', 'tp')
- gate_row_square: float32 [8, 2048], P('ep')
- up_row_square: float32 [8, 2048], P('ep')
- down_row_square: float32 [8, 3072], P('ep', 'tp')
Inputs may be any that keep to these rules, and one draw needn't show every extreme that they name: `routing`: each token names 2 different experts. Among the 128 rows of one device no expert is named more than 48 times; some device reaches 48. `gate_weights`: each row is positive and sums to one up to rounding.
All inputs are finite; a program needn't handle non-finite values.
Results may differ from a plain program's by a relative error of at most 0.015.
Values may be sent and summed in bfloat16 or wider, within the bound.
A program may use at most 64 MiB of HBM per device.

v0:
```python
import jax
import jax.numpy as jnp
from jax import lax
from jax.sharding import PartitionSpec as P


def matmul_tn(left_side, right_side):
    return lax.dot_general(
        left_side, right_side, (((0,), (0,)), ((), ())), preferred_element_type=jnp.float32
    )


def matmul_nt(left_side, right_side):
    return lax.dot_general(
        left_side, right_side, (((1,), (1,)), ((), ())), preferred_element_type=jnp.float32
    )


def slot_table(routing, experts, capacity):
    flat_routes = routing.reshape(-1)
    labels = lax.broadcasted_iota(jnp.int32, (flat_routes.shape[0], experts), 1)
    hit_mask = (flat_routes[:, None] == labels).astype(jnp.int32)
    ranking = jnp.cumsum(hit_mask, axis=0) - 1
    position = jnp.sum(hit_mask * ranking, axis=1)
    slot_id = flat_routes * capacity + position
    slot_index = lax.broadcasted_iota(jnp.int32, (experts * capacity, flat_routes.shape[0]), 0)
    return slot_index == slot_id[None, :]


def shards(tokens, routing, gate_weights, cotangent, expert_gate, expert_up, expert_down, router):
    tok_rows, local_width = tokens.shape
    top_count = routing.shape[1]
    experts = router.shape[1]
    n_tp = lax.axis_size("tp")
    capacity = 3 * top_count * tok_rows // (2 * experts)
    slot_count = experts * capacity
    matches = slot_table(routing, experts, capacity)
    by_token = jnp.any(matches.reshape(slot_count, tok_rows, top_count), axis=2).astype(
        jnp.bfloat16
    )
    input_send = jnp.dot(by_token, tokens, preferred_element_type=jnp.float32).astype(jnp.bfloat16)
    tangent_send = jnp.dot(by_token, cotangent, preferred_element_type=jnp.float32).astype(
        jnp.bfloat16
    )
    weight_flat = gate_weights.reshape(-1).astype(jnp.float32)
    weight_send = jnp.sum(jnp.where(matches, weight_flat[None, :], 0.0), axis=1).astype(
        jnp.bfloat16
    )
    input_slots, tangent_slots, weight_slots = (
        lax.all_to_all(
            input_send.reshape(experts, capacity, local_width),
            "ep",
            split_axis=0,
            concat_axis=0,
            tiled=True,
        ),
        lax.all_to_all(
            tangent_send.reshape(experts, capacity, local_width),
            "ep",
            split_axis=0,
            concat_axis=0,
            tiled=True,
        ),
        lax.all_to_all(
            weight_send.reshape(experts, capacity), "ep", split_axis=0, concat_axis=0, tiled=True
        ),
    )
    input_slots = input_slots.reshape(slot_count, local_width)
    tangent_slots = tangent_slots.reshape(slot_count, local_width)
    slot_weight = weight_slots.reshape(slot_count, 1).astype(jnp.float32)
    gate_matrix = expert_gate[0]
    up_matrix = expert_up[0]
    down_matrix = expert_down[0]
    hidden_local = gate_matrix.shape[1]
    full_input, full_tangent = (
        lax.all_gather(input_slots, "tp", axis=1, tiled=True),
        lax.all_gather(tangent_slots, "tp", axis=1, tiled=True),
    )
    pre_gate = jnp.dot(full_input, gate_matrix, preferred_element_type=jnp.float32)
    pre_up = jnp.dot(full_input, up_matrix, preferred_element_type=jnp.float32)
    back_proj = matmul_nt(full_tangent, down_matrix)
    sigmoid_gate = jax.nn.sigmoid(pre_gate)
    active = pre_gate * sigmoid_gate
    hidden = active * pre_up
    slot_part = jnp.sum(hidden * back_proj, axis=1)
    scaled = (slot_weight * hidden).astype(jnp.bfloat16)
    hidden_grad = slot_weight * back_proj
    gate_pre_grad = (
        hidden_grad * pre_up * sigmoid_gate * (1.0 + pre_gate * (1.0 - sigmoid_gate))
    ).astype(jnp.bfloat16)
    up_pre_grad = (hidden_grad * active).astype(jnp.bfloat16)
    gate_sum = matmul_tn(full_input, gate_pre_grad)
    up_sum = matmul_tn(full_input, up_pre_grad)
    down_sum = matmul_tn(scaled, full_tangent)
    unit_count = hidden_local * n_tp
    slot_gate_grad, gate_square, up_square = lax.psum(
        (slot_part, jnp.sum(gate_sum * gate_sum, axis=1), jnp.sum(up_sum * up_sum, axis=1)), "tp"
    )
    slot_grad = lax.psum_scatter(
        (matmul_nt(gate_matrix, gate_pre_grad) + matmul_nt(up_matrix, up_pre_grad)).astype(
            jnp.bfloat16
        ),
        "tp",
        scatter_dimension=0,
        tiled=True,
    ).astype(jnp.float32)
    back_rows, back_gate = (
        lax.all_to_all(
            slot_grad.reshape(local_width, experts, capacity).astype(jnp.bfloat16),
            "ep",
            split_axis=1,
            concat_axis=1,
            tiled=True,
        ).astype(jnp.float32),
        lax.all_to_all(
            slot_gate_grad.reshape(1, experts, capacity).astype(jnp.bfloat16),
            "ep",
            split_axis=1,
            concat_axis=1,
            tiled=True,
        ).astype(jnp.float32),
    )
    back_flat = back_rows.reshape(local_width, slot_count)
    token_part = lax.dot_general(
        by_token.astype(jnp.float32),
        back_flat,
        (((0,), (1,)), ((), ())),
        precision=lax.Precision.HIGHEST,
        preferred_element_type=jnp.float32,
    )
    gate_grad = jnp.sum(jnp.where(matches, back_gate.reshape(slot_count, 1), 0.0), axis=0).reshape(
        tok_rows, top_count
    )
    weights_f = gate_weights.astype(jnp.float32)
    mixed_term = jnp.sum(weights_f * gate_grad, axis=1, keepdims=True)
    logit_grad = weights_f * (gate_grad - mixed_term)
    labels = lax.broadcasted_iota(jnp.int32, (1, 1, experts), 2)
    signal = jnp.sum(
        jnp.where(routing[:, :, None] == labels, logit_grad[:, :, None], 0.0), axis=1
    ).astype(jnp.bfloat16)
    router_term = matmul_tn(signal, tokens)
    router_grad = lax.psum_scatter(router_term, "ep", scatter_dimension=0, tiled=True)
    router_cols = lax.dynamic_slice_in_dim(
        router, lax.axis_index("tp") * local_width, local_width, 0
    )
    token_grad = token_part + matmul_nt(signal, router_cols)
    return (
        token_grad,
        gate_grad,
        gate_sum.astype(jnp.bfloat16)[None],
        up_sum.astype(jnp.bfloat16)[None],
        down_sum.astype(jnp.bfloat16)[None],
        router_grad,
        (gate_square / unit_count)[None, :],
        (up_square / unit_count)[None, :],
        jnp.mean(down_sum * down_sum, axis=1)[None, :],
    )


def solution(mesh):
    in_specs = (
        P("ep", "tp"),
        P("ep", None),
        P("ep", None),
        P("ep", "tp"),
        P("ep", None, "tp"),
        P("ep", None, "tp"),
        P("ep", "tp", None),
        P(),
    )
    out_specs = (
        P("ep", "tp"),
        P("ep", None),
        P("ep", None, "tp"),
        P("ep", None, "tp"),
        P("ep", "tp", None),
        P("ep", "tp"),
        P("ep", None),
        P("ep", None),
        P("ep", "tp"),
    )
    return jax.shard_map(shards, mesh=mesh, in_specs=in_specs, out_specs=out_specs, check_vma=False)
```

profile of v0, /device:TPU:0, one launch (start us, length us, event | category | flops | bytes accessed | tf_op | source)
XLA Modules:
  0.0 198.4 jit_solution(634867109841897890)
XLA Ops:
  11.6 19.2 %all_to_all.26 = bf16[8,48,512]{2,1,0:T(8,128)(2,1)} all-to-all(bf16[8,48,512]{2,1,0:T(8,128)(2,1)S(1)} %bitcast.63), channel_id=1, replica_groups=mesh['ep'=8,'tp'=4] {'ep'}, dimensions={0} | all-to-all | bytes 786432 | tf_op jit(solution)/shard_map/all_to_all | solution.py:50
  31.2 15.1 %all_to_all.27 = bf16[8,48,512]{2,1,0:T(8,128)(2,1)} all-to-all(bf16[8,48,512]{2,1,0:T(8,128)(2,1)S(1)} %bitcast.64), channel_id=1, replica_groups=mesh['ep'=8,'tp'=4] {'ep'}, dimensions={0} | all-to-all | bytes 786432 | tf_op jit(solution)/shard_map/all_to_all | solution.py:57
  46.3 3.1 %all-gather.5.cloned.1.call-done = bf16[384,2048]{1,0:T(8,128)(2,1)} async-done(((bf16[384,512]{1,0:T(8,128)(2,1)}), bf16[384,2048]{1,0:T(8,128)(2,1)}) %all-gather.5.cloned.1.call-update) | async-done | bytes 1572880 | tf_op jit(solution)/shard_map/all_gather | solution.py:76
  49.3 4.0 %fusion.2 = f32[384,768]{1,0:T(8,128)} fusion(bf16[384,2048]{1,0:T(8,128)(2,1)} %all-gather.5.cloned.1.call-done, bf16[1,2048,768]{2,1,0:T(8,128)(2,1)S(1)} %copy-done), kind=kOutput, calls=%fused_computation.5 | convolution fusion | flops 1207959552 | bytes 5898240 | tf_op jit(solution)/shard_map/dot_general | solution.py:79
  53.3 2.4 %fusion.6 = f32[384,768]{1,0:T(8,128)} fusion(bf16[384,2048]{1,0:T(8,128)(2,1)S(1)} %copy-done.13, bf16[1,2048,768]{2,1,0:T(8,128)(2,1)S(1)} %copy-done.11), kind=kOutput, calls=%fused_computation.9 | convolution fusion | flops 1207959552 | bytes 5898240 | tf_op jit(solution)/shard_map/dot_general | solution.py:80
  55.7 14.9 %all-gather.3.cloned.1.call-done = bf16[384,2048]{1,0:T(8,128)(2,1)} async-done(((bf16[384,512]{1,0:T(8,128)(2,1)}), bf16[384,2048]{1,0:T(8,128)(2,1)}) %all-gather.3.cloned.1.call-update) | async-done | bytes 1572880 | tf_op jit(solution)/shard_map/all_gather | solution.py:77
  70.6 5.5 %multiply_reduce_fusion.3 = (f32[384]{0:T(512)S(1)}, f32[384,768]{1,0:T(8,128)}) fusion(f32[384,768]{1,0:T(8,128)} %fusion.6, f32[384,768]{1,0:T(8,128)} %fusion.2, bf16[384,2048]{1,0:T(8,128)(2,1)} %all-gather.3.cloned.1.call-done, bf16[1,768,2048]{2,1,0:T(8,128)(2,1)} %param.14), kind=kOutput, calls=%fused_computation.21 | convolution fusion | flops 1210023552 | bytes 8259072 | tf_op jit(solution)/shard_map/dot_general | solution.py:14
  76.0 5.9 %psum.21 = bf16[384]{0:T(512)(128)(2,1)S(1)} all-reduce(f32[384]{0:T(512)S(1)} %get-tuple-element.75), channel_id=1, replica_groups=mesh['ep'=8,'tp'=4] {'tp'}, use_global_device_ids=true, to_apply=%region_7.8 | all-reduce | flops 384 | bytes 2304 | tf_op jit(solution)/shard_map/psum | solution.py:96
  82.6 5.7 %all-to-all-start.4 = ((bf16[1,8,48]{2,0,1:T(2,128)(2,1)}), bf16[1,8,48]{2,0,1:T(2,128)(2,1)S(1)}, u32[]{:S(2)}, u32[]{:S(2)}) async-start(bf16[1,8,48]{2,0,1:T(2,128)(2,1)} %convert_element_type.124), calls=%async_computation.5 | async-start | bytes 8192 | tf_op jit(solution)/shard_map/all_to_all | solution.py:115
  88.6 6.1 %all-to-all-done.4 = bf16[1,8,48]{2,0,1:T(2,128)(2,1)S(1)} async-done(((bf16[1,8,48]{2,0,1:T(2,128)(2,1)}), bf16[1,8,48]{2,0,1:T(2,128)(2,1)S(1)}, u32[]{:S(2)}, u32[]{:S(2)}) %all-to-all-start.4) | async-done | bytes 800 | tf_op jit(solution)/shard_map/all_to_all | solution.py:115
  95.1 8.9 %all_to_all.28 = bf16[8,1,48]{2,1,0:T(2,128)(2,1)S(1)} all-to-all(bf16[8,1,48]{2,1,0:T(2,128)(2,1)S(1)} %convert_element_type.123), channel_id=1, replica_groups=mesh['ep'=8,'tp'=4] {'ep'}, dimensions={0} | all-to-all | bytes 1536 | tf_op jit(solution)/shard_map/all_to_all | solution.py:64
  104.0 2.6 %multiply_convert_fusion.1 = (bf16[384,768]{1,0:T(8,128)(2,1)S(1)}, bf16[384,768]{1,0:T(8,128)(2,1)S(1)}) fusion(f32[384,768]{1,0:T(8,128)} %get-tuple-element.76, f32[384]{0:T(512)S(1)} %reshape.142, f32[384,768]{1,0:T(8,128)} %fusion.2, f32[384,768]{1,0:T(8,128)} %fusion.6), kind=kLoop, calls=%fused_computation.22 | loop fusion | flops 4128768 | bytes 4720128 | tf_op jit(solution)/shard_map/convert_element_type | solution.py:91
  106.6 1.4 fusion
  108.9 2.6 %fusion.12 = bf16[2048,384]{0,1:T(8,128)(2,1)} fusion(f32[384,2048]{1,0:T(8,128)S(1)} %fusion, bf16[384,768]{1,0:T(8,128)(2,1)S(1)} %get-tuple-element.73, bf16[1,2048,768]{2,1,0:T(8,128)(2,1)S(1)} %copy-done.12), kind=kOutput, calls=%fused_computation.17 | convolution fusion | flops 1209532416 | bytes 8454144 | tf_op jit(solution)/shard_map/dot_general | solution.py:14
  113.2 33.4 %all-reduce = f32[8,512]{1,0:T(8,128)S(1)} all-reduce(f32[8,512]{1,0:T(8,128)S(1)} %fusion.29), channel_id=3, replica_groups=mesh['ep'=8,'tp'=4] {'ep'}, use_global_device_ids=true, to_apply=%region_11.12.clone | all-reduce | flops 4096 | bytes 32768
  147.8 1.6 fusion.21
  149.4 5.2 %multiply_reduce_fusion.2 = (f32[2048]{0:T(1024)S(1)}, bf16[1,2048,768]{1,2,0:T(8,128)(2,1)}) fusion(bf16[384,2048]{1,0:T(8,128)(2,1)} %all-gather.5.cloned.1.call-done, bf16[384,768]{1,0:T(8,128)(2,1)} %copy-done.5), kind=kOutput, calls=%fused_computation.2 | convolution fusion | flops 1212676096 | bytes 5316608 | tf_op jit(solution)/shard_map/dot_general | solution.py:8
  154.6 3.7 %multiply_reduce_fusion = (f32[768]{0:T(1024)S(1)}, bf16[1,768,2048]{2,1,0:T(8,128)(2,1)}) fusion(bf16[384,2048]{1,0:T(8,128)(2,1)S(1)} %copy-done.14, f32[384]{0:T(512)S(1)} %reshape.142, f32[384,768]{1,0:T(8,128)S(1)} %copy-done.2, f32[384,768]{1,0:T(8,128)S(1)} %copy-done.1), kind=kOutput, calls=%fused_computation | convolution fusion | flops 1214741760 | bytes 7082496 | tf_op jit(solution)/shard_map/dot_general | solution.py:8
  158.3 3.5 %all-to-all-start.3 = ((bf16[512,8,48]{0,2,1:T(8,128)(2,1)}), bf16[512,8,48]{0,2,1:T(8,128)(2,1)S(1)}, u32[]{:S(2)}, u32[]{:S(2)}) async-start(bf16[512,8,48]{0,2,1:T(8,128)(2,1)} %bitcast.66), calls=%async_computation.4 | async-start | bytes 786432 | tf_op jit(solution)/shard_map/all_to_all | solution.py:108
  162.4 4.6 %copy.73 = bf16[1,2048,768]{2,1,0:T(8,128)(2,1)} copy(bf16[1,2048,768]{1,2,0:T(8,128)(2,1)} %get-tuple-element.72) | data formatting | bytes 6291456
  167.0 5.7 %multiply_reduce_fusion.1 = (f32[2048]{0:T(1024)}, bf16[1,2048,768]{1,2,0:T(8,128)(2,1)}) fusion(bf16[384,2048]{1,0:T(8,128)(2,1)} %all-gather.5.cloned.1.call-done, bf16[384,768]{1,0:T(8,128)(2,1)} %copy-done.4), kind=kOutput, calls=%fused_computation.1 | convolution fusion | flops 1212676096 | bytes 5316608 | tf_op jit(solution)/shard_map/dot_general | solution.py:8
  172.7 4.6 %copy.74 = bf16[1,2048,768]{2,1,0:T(8,128)(2,1)} copy(bf16[1,2048,768]{1,2,0:T(8,128)(2,1)} %get-tuple-element.70) | data formatting | bytes 6291456
  177.3 11.3 %all-reduce.1 = (f32[2048]{0:T(1024)}, f32[2048]{0:T(1024)}) all-reduce(f32[2048]{0:T(1024)S(1)} %get-tuple-element.71, f32[2048]{0:T(1024)} %get-tuple-element.69), channel_id=1, replica_groups=mesh['ep'=8,'tp'=4] {'tp'}, use_global_device_ids=true, to_apply=%region_13.14 | all-reduce | flops 4096 | bytes 32768 | tf_op jit(solution)/shard_map/psum | solution.py:96
  189.9 2.0 convolution_add_fusion
  (76 shorter events, 11.8 us)
Async XLA Ops:
  7.2 42.2 %copy-start = (bf16[1,2048,768]{2,1,0:T(8,128)(2,1)S(1)}, bf16[1,2048,768]{2,1,0:T(8,128)(2,1)}, u32[]{:S(2)}) copy-start(bf16[1,2048,768]{2,1,0:T(8,128)(2,1)} %param.12) | copy-start | bytes 9437188
  7.2 23.7 %copy-start.7 = (bf16[128,512]{1,0:T(8,128)(2,1)S(1)}, bf16[128,512]{1,0:T(8,128)(2,1)}, u32[]{:S(2)}) copy-start(bf16[128,512]{1,0:T(8,128)(2,1)} %param.11) | copy-start | bytes 393220
  7.2 42.1 %all-gather.5.cloned.1.call-start = ((), (), s32[]{:S(2)}) async-start(), calls=%async_computation.7 | async-start | bytes 1966080 | tf_op jit(solution)/shard_map/all_gather | solution.py:76
  10.4 35.9 %copy-start.3 = (pred[384,128]{1,0:T(8,128)(4,1)}, pred[384,128]{1,0:T(8,128)(4,1)S(1)}, u32[]{:S(2)}) copy-start(pred[384,128]{1,0:T(8,128)(4,1)S(1)} %fusion.19) | copy-start | bytes 147460
  30.8 39.7 %all-gather.3.cloned.1.call-start = ((), (), s32[]{:S(2)}) async-start(), calls=%async_computation.6 | async-start | bytes 1966080 | tf_op jit(solution)/shard_map/all_gather | solution.py:77
  49.3 4.0 %copy-start.11 = (bf16[1,2048,768]{2,1,0:T(8,128)(2,1)S(1)}, bf16[1,2048,768]{2,1,0:T(8,128)(2,1)}, u32[]{:S(2)}) copy-start(bf16[1,2048,768]{2,1,0:T(8,128)(2,1)} %param.13) | copy-start | bytes 9437188
  49.3 4.0 %copy-start.13 = (bf16[384,2048]{1,0:T(8,128)(2,1)S(1)}, bf16[384,2048]{1,0:T(8,128)(2,1)}, u32[]{:S(2)}) copy-start(bf16[384,2048]{1,0:T(8,128)(2,1)} %all-gather.5.cloned.1.call-done) | copy-start | bytes 4718596
  55.7 32.6 %copy-start.10 = (bf16[128,2]{0,1:T(2,128)(2,1)S(1)}, bf16[128,2]{0,1:T(2,128)(2,1)}, u32[]{:S(2)}) copy-start(bf16[128,2]{0,1:T(2,128)(2,1)} %param.10) | copy-start | bytes 1540
  82.6 12.1 %all-to-all-start.4 = ((bf16[1,8,48]{2,0,1:T(2,128)(2,1)}), bf16[1,8,48]{2,0,1:T(2,128)(2,1)S(1)}, u32[]{:S(2)}, u32[]{:S(2)}) async-start(bf16[1,8,48]{2,0,1:T(2,128)(2,1)} %convert_element_type.124), calls=%async_computation.5 | async-start | bytes 8192 | tf_op jit(solution)/shard_map/all_to_all | solution.py:115
  88.3 70.1 %reduce-scatter.2.cloned.1.call-start = ((), (), s32[]{:S(2)}) async-start(), calls=%async_computation.8 | async-start | bytes 1966080 | tf_op jit(solution)/shard_map/reduce_scatter | solution.py:99
  106.6 1.5 copy-start.5
  106.6 1.5 copy-start.4
  106.6 2.3 %copy-start.12 = (bf16[1,2048,768]{2,1,0:T(8,128)(2,1)S(1)}, bf16[1,2048,768]{2,1,0:T(8,128)(2,1)}, u32[]{:S(2)}) copy-start(bf16[1,2048,768]{2,1,0:T(8,128)(2,1)} %param.13) | copy-start | bytes 9437188
  111.5 0.7 copy-start.15
  111.5 1.5 copy-start.9
  111.5 1.5 copy-start.6
  112.9 41.7 %copy-start.8 = (f32[128,2]{0,1:T(2,128)}, f32[128,2]{0,1:T(2,128)S(1)}, u32[]{:S(2)}) copy-start(f32[128,2]{0,1:T(2,128)S(1)} %copy.71) | copy-start | bytes 3076
  149.4 5.2 %copy-start.1 = (f32[384,768]{1,0:T(8,128)S(1)}, f32[384,768]{1,0:T(8,128)}, u32[]{:S(2)}) copy-start(f32[384,768]{1,0:T(8,128)} %fusion.2) | copy-start | bytes 3538948
  149.4 5.2 %copy-start.2 = (f32[384,768]{1,0:T(8,128)S(1)}, f32[384,768]{1,0:T(8,128)}, u32[]{:S(2)}) copy-start(f32[384,768]{1,0:T(8,128)} %fusion.6) | copy-start | bytes 3538948
  149.4 5.2 %copy-start.14 = (bf16[384,2048]{1,0:T(8,128)(2,1)S(1)}, bf16[384,2048]{1,0:T(8,128)(2,1)}, u32[]{:S(2)}) copy-start(bf16[384,2048]{1,0:T(8,128)(2,1)} %all-gather.3.cloned.1.call-done) | copy-start | bytes 4718596
  158.3 31.6 %all-to-all-start.3 = ((bf16[512,8,48]{0,2,1:T(8,128)(2,1)}), bf16[512,8,48]{0,2,1:T(8,128)(2,1)S(1)}, u32[]{:S(2)}, u32[]{:S(2)}) async-start(bf16[512,8,48]{0,2,1:T(8,128)(2,1)} %bitcast.66), calls=%async_computation.4 | async-start | bytes 786432 | tf_op jit(solution)/shard_map/all_to_all | solution.py:108
Sparse Core Ops, SparseCore 0:
  31.0 18.3 all-gather.4
  50.9 19.6 all-gather.2
  111.7 25.3 reduce-scatter.1
where the time goes:
time: 199 us; the launch traced here: 198 us
  blocking collectives  93.7 us (47%)
  matrix products  35.5 us (18%)
  waiting for transfers between devices  24.1 us (12%)
  local copies, waits for them, and re-layouts  16.2 us (8%)
  between operations  14 us (7%)
  starting transfers between devices  9.23 us (5%)
  other arithmetic  5.67 us (3%)
    unnamed x1, blocking collectives  33.4 us
    all_to_all x1, blocking collectives, shards(): lax.all_to_all(input_send.reshape(experts, capacity, local_width), 'ep',...  19.2 us
    psum x2, blocking collectives, shards(): lax.psum((slot_part, jnp.sum(gate_sum * gate_sum, axis=1), jnp.sum(up_sum...  17.1 us
    all_to_all x1, blocking collectives, shards(): lax.all_to_all(tangent_send.reshape(experts, capacity, local_width), 'ep'...  15.1 us
    all_gather x1, waiting for transfers between devices, shards(): lax.all_gather(tangent_slots, 'tp', axis=1, tiled=True)  14.9 us
    dot_general x4, matrix products, matmul_tn(): lax.dot_general(left_side, right_side, (((0,), (0,)), ((), ())), preferre...  14.7 us
    unnamed x37, local copies, waits for them, and re-layouts  13.6 us
    dot_general x4, matrix products, matmul_nt(): lax.dot_general(left_side, right_side, (((1,), (1,)), ((), ())), preferre...  11.1 us
  transfers between devices with their start and end apart: 5, of which 3 were waited for; matrix products, arithmetic and copies ran while one was open for 18% of the time, Pallas kernels for 0%

commit v1 on v0

v1 whole, which is shorter than its diff:
```python
import functools

import jax
import jax.numpy as jnp
from jax import lax
from jax.experimental import pallas as pl
from jax.experimental.pallas import tpu as pltpu
from jax.sharding import PartitionSpec as P

MESH = pl.DeviceIdType.MESH
F32 = jnp.float32
BF16 = jnp.bfloat16


def matmul_tn(left_side, right_side):
    return lax.dot_general(
        left_side, right_side, (((0,), (0,)), ((), ())), preferred_element_type=F32
    )


def matmul_nt(left_side, right_side):
    return lax.dot_general(
        left_side, right_side, (((1,), (1,)), ((), ())), preferred_element_type=F32
    )


def loop(lower, upper, body):
    if upper - lower <= 8:
        for i in range(lower, upper):
            body(i)
    else:
        lax.fori_loop(lower, upper, lambda i, carry: (body(i), carry)[1], 0)


def place():
    ep, tp = lax.axis_index("ep"), lax.axis_index("tp")
    return ep, tp, lax.div(tp, 2), lax.rem(tp, 2)


def greet(n_ep, n_tp, all_tp):
    ep, tp, y, core = place()
    barrier = pltpu.get_barrier_semaphore()

    def to_ep(r):
        pl.semaphore_signal(
            barrier, inc=1, device_id=(lax.rem(ep + r, n_ep), tp), device_id_type=MESH
        )

    def to_tp(r):
        pl.semaphore_signal(
            barrier, inc=1, device_id=(ep, lax.rem(tp + r, n_tp)), device_id_type=MESH
        )

    def to_y(r):
        other = lax.rem(y + r, n_tp // 2) * 2 + core
        pl.semaphore_signal(barrier, inc=1, device_id=(ep, other), device_id_type=MESH)

    loop(1, n_ep, to_ep)
    if all_tp:
        loop(1, n_tp, to_tp)
        pl.semaphore_wait(barrier, n_ep - 1 + n_tp - 1)
    else:
        loop(1, n_tp // 2, to_y)
        pl.semaphore_signal(
            barrier, inc=1, device_id=(ep, y * 2 + 1 - core), device_id_type=MESH
        )
        pl.semaphore_wait(barrier, n_ep - 1 + n_tp // 2)


def dispatch_kernel(
    n_ep,
    n_tp,
    chunks,
    x_ref,
    t_ref,
    w_ref,
    ox_ref,
    ot_ref,
    ow_ref,
    ep_send,
    ep_recv,
    y_send,
    y_recv,
    core_send,
    core_recv,
    own_sem,
):
    ep, tp, y, core = place()
    n_y = n_tp // 2
    width = x_ref.shape[2]
    per = n_ep // chunks
    partner = y * 2 + 1 - core
    greet(n_ep, n_tp, False)
    sources = (x_ref, t_ref)
    outs = (ox_ref, ot_ref)

    def cols(which):
        return pl.ds(pl.multiple_of(which * width, width), width)

    def ep_copy(which, dst, src):
        if which == 2:
            return pltpu.make_async_remote_copy(
                src_ref=w_ref.at[dst],
                dst_ref=ow_ref.at[src],
                send_sem=ep_send.at[2, dst],
                recv_sem=ep_recv.at[2, src],
                device_id=(dst, tp),
                device_id_type=MESH,
            )
        return pltpu.make_async_remote_copy(
            src_ref=sources[which].at[dst],
            dst_ref=outs[which].at[src, :, cols(tp)],
            send_sem=ep_send.at[which, dst],
            recv_sem=ep_recv.at[which, src],
            device_id=(dst, tp),
            device_id_type=MESH,
        )

    def y_copy(which, source_y, target_y, chunk):
        piece = outs[which].at[pl.ds(chunk * per, per), :, cols(source_y * 2 + core)]
        return pltpu.make_async_remote_copy(
            src_ref=piece,
            dst_ref=piece,
            send_sem=y_send.at[which, target_y, chunk],
            recv_sem=y_recv.at[which, source_y, chunk],
            device_id=(ep, target_y * 2 + core),
            device_id_type=MESH,
        )

    def core_copy(which, source_y, source_core, chunk):
        piece = outs[which].at[pl.ds(chunk * per, per), :, cols(source_y * 2 + source_core)]
        return pltpu.make_async_remote_copy(
            src_ref=piece,
            dst_ref=piece,
            send_sem=core_send.at[which, source_y, chunk],
            recv_sem=core_recv.at[which, source_y, chunk],
            device_id=(ep, partner),
            device_id_type=MESH,
        )

    def own_copy(which):
        if which == 2:
            return pltpu.make_async_copy(w_ref.at[ep], ow_ref.at[ep], own_sem.at[2])
        return pltpu.make_async_copy(
            sources[which].at[ep], outs[which].at[ep, :, cols(tp)], own_sem.at[which]
        )

    for which in range(3):
        own_copy(which).start()

    def send(r):
        for which in range(3):
            ep_copy(which, lax.rem(ep + r, n_ep), ep).start()

    loop(1, n_ep, send)
    for which in range(3):
        own_copy(which).wait()
    my_chunk = lax.div(ep, per)

    def chunk_at(j):
        return lax.rem(my_chunk - j + chunks, chunks)

    def relay(j):
        chunk = chunk_at(j)
        for which in range(2):
            for i in range(per):
                source = chunk * per + i

                @pl.when(source != ep)
                def _():
                    ep_copy(which, ep, source).wait_recv()

            for r in range(1, n_y):
                y_copy(which, y, lax.rem(y + r, n_y), chunk).start()
            core_copy(which, y, core, chunk).start()

    loop(0, chunks, relay)

    def forward(j):
        chunk = chunk_at(j)
        for r in range(1, n_y):
            source_y = lax.rem(y + n_y - r, n_y)
            for which in range(2):
                y_copy(which, source_y, y, chunk).wait_recv()
                core_copy(which, source_y, core, chunk).start()

    loop(0, chunks, forward)

    def finish(j):
        chunk = chunk_at(j)
        for which in range(2):
            for r in range(n_y):
                core_copy(which, r, 1 - core, chunk).wait_recv()
                core_copy(which, r, core, chunk).wait_send()
            for r in range(1, n_y):
                y_copy(which, y, lax.rem(y + r, n_y), chunk).wait_send()

    loop(0, chunks, finish)

    def drain(r):
        other = lax.rem(ep + r, n_ep)
        for which in range(3):
            ep_copy(which, other, ep).wait_send()
        ep_copy(2, ep, other).wait_recv()

    loop(1, n_ep, drain)


def dispatch(input_send, tangent_send, weight_send, n_ep, n_tp):
    _, cap, width = input_send.shape
    chunks = n_ep if n_ep <= 8 else next(c for c in range(8, 0, -1) if n_ep % c == 0)
    n_y = n_tp // 2
    dma = pltpu.SemaphoreType.DMA
    return pl.pallas_call(
        functools.partial(dispatch_kernel, n_ep, n_tp, chunks),
        out_shape=(
            jax.ShapeDtypeStruct((n_ep, cap, width * n_tp), BF16),
            jax.ShapeDtypeStruct((n_ep, cap, width * n_tp), BF16),
            jax.ShapeDtypeStruct(weight_send.shape, F32),
        ),
        in_specs=[pl.BlockSpec(memory_space=pltpu.VMEM)] * 3,
        out_specs=[pl.BlockSpec(memory_space=pltpu.VMEM)] * 3,
        scratch_shapes=[
            dma((3, n_ep)),
            dma((3, n_ep)),
            dma((2, n_y, chunks)),
            dma((2, n_y, chunks)),
            dma((2, n_y, chunks)),
            dma((2, n_y, chunks)),
            dma((3,)),
        ],
        compiler_params=pltpu.CompilerParams(collective_id=0, has_side_effects=True),
        name="dispatch",
    )(input_send, tangent_send, weight_send)


def return_kernel(
    n_ep,
    n_tp,
    chunks,
    part_ref,
    gate_ref,
    back_ref,
    back_gate_ref,
    core_buf,
    y_out,
    y_buf,
    ep_out,
    gate_buf,
    gate_out,
    core_send,
    core_recv,
    y_send,
    y_recv,
    ep_send,
    ep_recv,
    tp_send,
    tp_recv,
    gate_send,
    gate_recv,
    own_sem,
):
    ep, tp, y, core = place()
    n_y = n_tp // 2
    width = back_ref.shape[2]
    per = n_ep // chunks
    partner = y * 2 + 1 - core
    greet(n_ep, n_tp, True)

    def cols(which):
        return pl.ds(pl.multiple_of(which * width, width), width)

    def rows(chunk):
        return pl.ds(chunk * per, per)

    def core_copy(target_y, chunk):
        return pltpu.make_async_remote_copy(
            src_ref=part_ref.at[rows(chunk), :, cols(target_y * 2 + 1 - core)],
            dst_ref=core_buf.at[target_y, rows(chunk)],
            send_sem=core_send.at[target_y, chunk],
            recv_sem=core_recv.at[target_y, chunk],
            device_id=(ep, partner),
            device_id_type=MESH,
        )

    def y_copy(source_y, target_y, chunk):
        return pltpu.make_async_remote_copy(
            src_ref=y_out.at[target_y, rows(chunk)],
            dst_ref=y_buf.at[source_y, rows(chunk)],
            send_sem=y_send.at[target_y, chunk],
            recv_sem=y_recv.at[source_y, chunk],
            device_id=(ep, target_y * 2 + core),
            device_id_type=MESH,
        )

    def ep_copy(dst, src):
        return pltpu.make_async_remote_copy(
            src_ref=ep_out.at[dst],
            dst_ref=back_ref.at[src],
            send_sem=ep_send.at[dst],
            recv_sem=ep_recv.at[src],
            device_id=(dst, tp),
            device_id_type=MESH,
        )

    def tp_copy(dst, src):
        return pltpu.make_async_remote_copy(
            src_ref=gate_ref,
            dst_ref=gate_buf.at[src],
            send_sem=tp_send.at[dst],
            recv_sem=tp_recv.at[src],
            device_id=(ep, dst),
            device_id_type=MESH,
        )

    def gate_copy(dst, src):
        return pltpu.make_async_remote_copy(
            src_ref=gate_out.at[dst],
            dst_ref=back_gate_ref.at[src],
            send_sem=gate_send.at[dst],
            recv_sem=gate_recv.at[src],
            device_id=(dst, tp),
            device_id_type=MESH,
        )

    first = lax.div(ep, per)

    def chunk_at(j):
        return lax.rem(first + j, chunks)

    loop(1, n_tp, lambda r: tp_copy(lax.rem(tp + r, n_tp), tp).start())

    def start(j):
        for r in range(n_y):
            core_copy(lax.rem(y + r + 1, n_y), chunk_at(j)).start()

    loop(1, chunks + 1, start)

    def across(j):
        chunk = chunk_at(j)
        for r in range(1, n_y):
            target = lax.rem(y + r, n_y)
            core_copy(target, chunk).wait_recv()
            for i in range(per):
                at = chunk * per + i
                mine = part_ref[at, :, cols(target * 2 + core)].astype(F32)
                y_out[target, at] = (mine + core_buf[target, at].astype(F32)).astype(BF16)
            y_copy(y, target, chunk).start()

    loop(1, chunks + 1, across)

    total = gate_ref[...]
    for r in range(1, n_tp):
        source = lax.rem(tp + r, n_tp)
        tp_copy(tp, source).wait_recv()
        total = total + gate_buf[source]
    gate_out[...] = total
    loop(1, n_ep, lambda r: gate_copy(lax.rem(ep + r, n_ep), ep).start())
    own_gate = pltpu.make_async_copy(gate_out.at[ep], back_gate_ref.at[ep], own_sem.at[0])
    own_gate.start()

    def scatter(j):
        chunk = chunk_at(j)
        core_copy(y, chunk).wait_recv()
        for r in range(1, n_y):
            y_copy(lax.rem(y + r, n_y), y, chunk).wait_recv()
        for i in range(per):
            at = chunk * per + i
            value = part_ref[at, :, cols(tp)].astype(F32) + core_buf[y, at].astype(F32)
            for r in range(1, n_y):
                value = value + y_buf[lax.rem(y + r, n_y), at].astype(F32)
            ep_out[at] = value.astype(BF16)

            @pl.when(at != ep)
            def _():
                ep_copy(at, ep).start()

    loop(1, chunks + 1, scatter)
    own_rows = pltpu.make_async_copy(ep_out.at[ep], back_ref.at[ep], own_sem.at[1])
    own_rows.start()

    def drain(r):
        other = lax.rem(ep + r, n_ep)
        gate_copy(ep, other).wait_recv()
        gate_copy(other, ep).wait_send()
        ep_copy(ep, other).wait_recv()
        ep_copy(other, ep).wait_send()

    loop(1, n_ep, drain)
    loop(1, n_tp, lambda r: tp_copy(lax.rem(tp + r, n_tp), tp).wait_send())

    def finish(chunk):
        for r in range(n_y):
            core_copy(r, chunk).wait_send()
        for r in range(1, n_y):
            y_copy(y, lax.rem(y + r, n_y), chunk).wait_send()

    loop(0, chunks, finish)
    own_gate.wait()
    own_rows.wait()


def return_rows(part, gate_part, n_ep, n_tp):
    _, cap, features = part.shape
    width = features // n_tp
    chunks = n_ep if n_ep <= 8 else next(c for c in range(8, 0, -1) if n_ep % c == 0)
    n_y = n_tp // 2
    dma = pltpu.SemaphoreType.DMA
    return pl.pallas_call(
        functools.partial(return_kernel, n_ep, n_tp, chunks),
        out_shape=(
            jax.ShapeDtypeStruct((n_ep, cap, width), BF16),
            jax.ShapeDtypeStruct(gate_part.shape, F32),
        ),
        in_specs=[pl.BlockSpec(memory_space=pltpu.VMEM)] * 2,
        out_specs=[pl.BlockSpec(memory_space=pltpu.VMEM)] * 2,
        scratch_shapes=[
            pltpu.VMEM((n_y, n_ep, cap, width), BF16),
            pltpu.VMEM((n_y, n_ep, cap, width), BF16),
            pltpu.VMEM((n_y, n_ep, cap, width), BF16),
            pltpu.VMEM((n_ep, cap, width), BF16),
            pltpu.VMEM((n_tp,) + gate_part.shape, F32),
            pltpu.VMEM(gate_part.shape, F32),
            dma((n_y, chunks)),
            dma((n_y, chunks)),
            dma((n_y, chunks)),
            dma((n_y, chunks)),
            dma((n_ep,)),
            dma((n_ep,)),
            dma((n_tp,)),
            dma((n_tp,)),
            dma((n_ep,)),
            dma((n_ep,)),
            dma((2,)),
        ],
        compiler_params=pltpu.CompilerParams(collective_id=1, has_side_effects=True),
        name="return_rows",
    )(part, gate_part)


def sums_kernel(
    n_ep,
    n_tp,
    square_ref,
    term_ref,
    square_out,
    term_out,
    square_buf,
    term_buf,
    tp_send,
    tp_recv,
    ep_send,
    ep_recv,
):
    ep, tp, _, _ = place()
    greet(n_ep, n_tp, True)

    def tp_copy(dst, src):
        return pltpu.make_async_remote_copy(
            src_ref=square_ref,
            dst_ref=square_buf.at[src],
            send_sem=tp_send.at[dst],
            recv_sem=tp_recv.at[src],
            device_id=(ep, dst),
            device_id_type=MESH,
        )

    def ep_copy(dst, src):
        return pltpu.make_async_remote_copy(
            src_ref=term_ref.at[dst],
            dst_ref=term_buf.at[src],
            send_sem=ep_send.at[dst],
            recv_sem=ep_recv.at[src],
            device_id=(dst, tp),
            device_id_type=MESH,
        )

    loop(1, n_ep, lambda r: ep_copy(lax.rem(ep + r, n_ep), ep).start())
    loop(1, n_tp, lambda r: tp_copy(lax.rem(tp + r, n_tp), tp).start())
    square = square_ref[...]
    for r in range(1, n_tp):
        source = lax.rem(tp + r, n_tp)
        tp_copy(tp, source).wait_recv()
        square = square + square_buf[source]
    square_out[...] = square
    term_out[...] = term_ref[ep]

    def add(r):
        source = lax.rem(ep + r, n_ep)
        ep_copy(ep, source).wait_recv()
        term_out[...] += term_buf[source]

    loop(1, n_ep, add)
    loop(1, n_ep, lambda r: ep_copy(lax.rem(ep + r, n_ep), ep).wait_send())
    loop(1, n_tp, lambda r: tp_copy(lax.rem(tp + r, n_tp), tp).wait_send())


def small_sums(square, term, n_ep, n_tp):
    dma = pltpu.SemaphoreType.DMA
    return pl.pallas_call(
        functools.partial(sums_kernel, n_ep, n_tp),
        out_shape=(
            jax.ShapeDtypeStruct(square.shape, F32),
            jax.ShapeDtypeStruct(term.shape[1:], F32),
        ),
        in_specs=[pl.BlockSpec(memory_space=pltpu.VMEM)] * 2,
        out_specs=[pl.BlockSpec(memory_space=pltpu.VMEM)] * 2,
        scratch_shapes=[
            pltpu.VMEM((n_tp,) + square.shape, F32),
            pltpu.VMEM(term.shape, F32),
            dma((n_tp,)),
            dma((n_tp,)),
            dma((n_ep,)),
            dma((n_ep,)),
        ],
        compiler_params=pltpu.CompilerParams(collective_id=2, has_side_effects=True),
        name="small_sums",
    )(square, term)


def slot_table(routing, experts, capacity):
    flat_routes = routing.reshape(-1)
    labels = lax.broadcasted_iota(jnp.int32, (flat_routes.shape[0], experts), 1)
    hit_mask = (flat_routes[:, None] == labels).astype(jnp.int32)
    ranking = jnp.cumsum(hit_mask, axis=0) - 1
    position = jnp.sum(hit_mask * ranking, axis=1)
    slot_id = flat_routes * capacity + position
    slot_index = lax.broadcasted_iota(jnp.int32, (experts * capacity, flat_routes.shape[0]), 0)
    return slot_index == slot_id[None, :]


def lanes(slot_values, experts, capacity):
    padded = -(-capacity // 128) * 128
    rows = jnp.pad(slot_values.reshape(experts, 1, capacity), ((0, 0), (0, 7), (0, padded - capacity)))
    return rows


def shards(tokens, routing, gate_weights, cotangent, expert_gate, expert_up, expert_down, router):
    tok_rows, local_width = tokens.shape
    top_count = routing.shape[1]
    experts = router.shape[1]
    n_tp = lax.axis_size("tp")
    n_ep = lax.axis_size("ep")
    capacity = 3 * top_count * tok_rows // (2 * experts)
    slot_count = experts * capacity
    features = local_width * n_tp
    matches = slot_table(routing, experts, capacity)
    by_token = jnp.any(matches.reshape(slot_count, tok_rows, top_count), axis=2).astype(BF16)
    input_send = jnp.dot(by_token, tokens, preferred_element_type=F32).astype(BF16)
    tangent_send = jnp.dot(by_token, cotangent, preferred_element_type=F32).astype(BF16)
    weight_flat = gate_weights.reshape(-1).astype(F32)
    weight_send = jnp.sum(jnp.where(matches, weight_flat[None, :], 0.0), axis=1)
    full_input, full_tangent, weight_slots = dispatch(
        input_send.reshape(experts, capacity, local_width),
        tangent_send.reshape(experts, capacity, local_width),
        lanes(weight_send, experts, capacity),
        n_ep,
        n_tp,
    )
    full_input = full_input.reshape(slot_count, features)
    full_tangent = full_tangent.reshape(slot_count, features)
    slot_weight = weight_slots[:, 0, :capacity].reshape(slot_count, 1)
    gate_matrix = expert_gate[0]
    up_matrix = expert_up[0]
    down_matrix = expert_down[0]
    hidden_local = gate_matrix.shape[1]
    pre_gate = jnp.dot(full_input, gate_matrix, preferred_element_type=F32)
    pre_up = jnp.dot(full_input, up_matrix, preferred_element_type=F32)
    back_proj = matmul_nt(full_tangent, down_matrix)
    sigmoid_gate = jax.nn.sigmoid(pre_gate)
    active = pre_gate * sigmoid_gate
    hidden = active * pre_up
    slot_part = jnp.sum(hidden * back_proj, axis=1)
    scaled = (slot_weight * hidden).astype(BF16)
    hidden_grad = slot_weight * back_proj
    gate_pre_grad = (
        hidden_grad * pre_up * sigmoid_gate * (1.0 + pre_gate * (1.0 - sigmoid_gate))
    ).astype(BF16)
    up_pre_grad = (hidden_grad * active).astype(BF16)
    gate_sum = matmul_tn(full_input, gate_pre_grad)
    up_sum = matmul_tn(full_input, up_pre_grad)
    down_sum = matmul_tn(scaled, full_tangent)
    unit_count = hidden_local * n_tp
    slot_grad = (
        matmul_nt(gate_pre_grad, gate_matrix) + matmul_nt(up_pre_grad, up_matrix)
    ).astype(BF16)
    back_rows, back_gate = return_rows(
        slot_grad.reshape(experts, capacity, features),
        lanes(slot_part, experts, capacity),
        n_ep,
        n_tp,
    )
    back_flat = back_rows.reshape(slot_count, local_width)
    token_part = matmul_tn(by_token, back_flat)
    gate_slots = back_gate[:, 0, :capacity].reshape(slot_count, 1)
    gate_grad = jnp.sum(jnp.where(matches, gate_slots, 0.0), axis=0).reshape(tok_rows, top_count)
    weights_f = gate_weights.astype(F32)
    mixed_term = jnp.sum(weights_f * gate_grad, axis=1, keepdims=True)
    logit_grad = weights_f * (gate_grad - mixed_term)
    labels = lax.broadcasted_iota(jnp.int32, (1, 1, experts), 2)
    signal = jnp.sum(
        jnp.where(routing[:, :, None] == labels, logit_grad[:, :, None], 0.0), axis=1
    ).astype(BF16)
    router_term = matmul_tn(signal, tokens)
    squares = jnp.stack([jnp.sum(gate_sum * gate_sum, axis=1), jnp.sum(up_sum * up_sum, axis=1)])
    squares, router_grad = small_sums(squares, router_term[:, None, :], n_ep, n_tp)
    router_cols = lax.dynamic_slice_in_dim(
        router, lax.axis_index("tp") * local_width, local_width, 0
    )
    token_grad = token_part + matmul_nt(signal, router_cols)
    return (
        token_grad,
        gate_grad,
        gate_sum.astype(BF16)[None],
        up_sum.astype(BF16)[None],
        down_sum.astype(BF16)[None],
        router_grad,
        squares[0:1] / unit_count,
        squares[1:2] / unit_count,
        jnp.mean(down_sum * down_sum, axis=1)[None, :],
    )


def solution(mesh):
    in_specs = (
        P("ep", "tp"),
        P("ep", None),
        P("ep", None),
        P("ep", "tp"),
        P("ep", None, "tp"),
        P("ep", None, "tp"),
        P("ep", "tp", None),
        P(),
    )
    out_specs = (
        P("ep", "tp"),
        P("ep", None),
        P("ep", None, "tp"),
        P("ep", None, "tp"),
        P("ep", "tp", None),
        P("ep", "tp"),
        P("ep", None),
        P("ep", None),
        P("ep", "tp"),
    )
    return jax.shard_map(shards, mesh=mesh, in_specs=in_specs, out_specs=out_specs, check_vma=False)
```

time: 199 us -> 123 us (0.62)
  blocking collectives: 93.7 us -> 0 us
  Pallas kernels: 0 us -> 67.7 us
  waiting for transfers between devices: 24.1 us -> 0 us
  between operations: 14 us -> 0.88 us
  starting transfers between devices: 9.23 us -> 0 us
  matrix products: 35.5 us -> 31.6 us
    pallas_call x0 -> x3, Pallas kernels: none -> 67.7 us  [the longest x1 35.4 us: dispatch(): pl.pallas_call(functools.partial(dispatch_kernel, n_ep, n_tp, chunks), ou...]
    all_to_all x3 -> x0, blocking collectives: 43.2 us -> none  [the longest x1 19.2 us: shards(): lax.all_to_all(input_send.reshape(experts, capacity, local_width), 'ep',...]
    unnamed x1 -> x0, blocking collectives: 33.4 us -> none
    all_gather x2 -> x0, waiting for transfers between devices: 17.9 us -> none  [the longest x1 14.9 us: shards(): lax.all_gather(tangent_slots, 'tp', axis=1, tiled=True)]
    psum x2 -> x0, blocking collectives: 17.1 us -> none  [shards(): lax.psum((slot_part, jnp.sum(gate_sum * gate_sum, axis=1), jnp.sum(up_sum...]
    all_to_all x2 -> x0, starting transfers between devices: 9.12 us -> none  [the longest x1 5.66 us: shards(): lax.all_to_all(slot_gate_grad.reshape(1, experts, capacity).astype(jnp.bf...]
    all_to_all x2 -> x0, waiting for transfers between devices: 6.09 us -> none  [the longest x1 6.09 us: shards(): lax.all_to_all(slot_gate_grad.reshape(1, experts, capacity).astype(jnp.bf...]
    convert_element_type x2 -> x0, other arithmetic: 2.58 us -> none  [the longest x1 2.57 us: shards(): up_pre_grad = (hidden_grad * active).astype(jnp.bfloat16)]
  transfers between devices with their start and end apart: 5 -> 0, of which waited for: 3 -> 0; matrix products, arithmetic and copies ran while one was open for 18% -> 0% of each run, Pallas kernels for 0% -> 0%
where the time goes in v1:
time: 123 us; the launch traced here: 122 us
  Pallas kernels  67.7 us (55%)
  matrix products  31.6 us (26%)
  local copies, waits for them, and re-layouts  17.9 us (15%)
  other arithmetic  3.86 us (3%)
    pallas_call x1, Pallas kernels, dispatch(): pl.pallas_call(functools.partial(dispatch_kernel, n_ep, n_tp, chunks), ou...  35.4 us
    pallas_call x1, Pallas kernels, return_rows(): pl.pallas_call(functools.partial(return_kernel, n_ep, n_tp, chunks), out_...  23.5 us
    dot_general x5, matrix products, matmul_tn(): lax.dot_general(left_side, right_side, (((0,), (0,)), ((), ())), preferre...  14.5 us
    unnamed x32, local copies, waits for them, and re-layouts  11.8 us
    dot_general x4, matrix products, matmul_nt(): lax.dot_general(left_side, right_side, (((1,), (1,)), ((), ())), preferre...  8.97 us
    pallas_call x1, Pallas kernels, small_sums(): pl.pallas_call(functools.partial(sums_kernel, n_ep, n_tp), out_shape=(jax...  8.81 us
    dot_general x1, matrix products, shards(): pre_gate = jnp.dot(full_input, gate_matrix, preferred_element_type=F32)  2.93 us

profile of v1, /device:TPU:0, one launch (start us, length us, event | category | flops | bytes accessed | tf_op | source)
XLA Modules:
  0.0 121.9 jit_solution(13027139817735637847)
XLA Ops:
  0.7 0.9 copy.41
  3.0 0.7 multiply_add_fusion.1
  3.8 0.8 copy.44
  5.0 0.6 pad.7.w_ref
  5.6 1.9 %convolution_convert_fusion = bf16[384,512]{1,0:T(8,128)(2,1)} fusion(pred[384,128]{1,0:T(8,128)(4,1)S(1)} %fusion.16, bf16[128,512]{1,0:T(8,128)(2,1)} %param.11), kind=kOutput, calls=%fused_computation.17 | convolution fusion | flops 50528256 | bytes 573440 | tf_op jit(solution)/shard_map/dot_general | solution.py:550
  7.5 1.9 %convolution_convert_fusion.1 = bf16[384,512]{1,0:T(8,128)(2,1)} fusion(pred[384,128]{1,0:T(8,128)(4,1)S(1)} %fusion.16, bf16[128,512]{1,0:T(8,128)(2,1)} %param.8), kind=kOutput, calls=%fused_computation.18 | convolution fusion | flops 50528256 | bytes 573440 | tf_op jit(solution)/shard_map/dot_general | solution.py:549
  9.4 35.4 %dispatch.1 = (bf16[8,48,2048]{2,1,0:T(8,128)(2,1)}, bf16[8,48,2048]{2,1,0:T(8,128)(2,1)}, f32[8,8,128]{2,1,0:T(8,128)}) custom-call(bf16[8,48,512]{2,1,0:T(8,128)(2,1)} %bitcast.58, bf16[8,48,512]{2,1,0:T(8,128)(2,1)} %bitcast.57, f32[8,8,128]{2,1,0:T(8,128)} %pad.7.w_ref), custom_call_target="tpu_custom_call" | custom-call | tf_op jit(solution)/shard_map/dispatch/pallas_call | solution.py:214
  44.8 0.8 slice_reduce_fusion.2
  45.6 2.9 %fusion.2 = f32[384,768]{1,0:T(8,128)S(1)} fusion(bf16[384,2048]{1,0:T(8,128)(2,1)} %bitcast.62, bf16[1,2048,768]{2,1,0:T(8,128)(2,1)S(1)} %copy-done), kind=kOutput, calls=%fused_computation.5 | convolution fusion | flops 1207959552 | bytes 5898240 | tf_op jit(solution)/shard_map/dot_general | solution.py:567
  48.6 1.4 %fusion.6 = f32[384,768]{1,0:T(8,128)S(1)} fusion(bf16[384,2048]{1,0:T(8,128)(2,1)S(1)} %bitcast.64, bf16[1,2048,768]{2,1,0:T(8,128)(2,1)S(1)} %copy-done.7), kind=kOutput, calls=%fused_computation.9 | convolution fusion | flops 1207959552 | bytes 5898240 | tf_op jit(solution)/shard_map/dot_general | solution.py:568
  51.0 2.9 %multiply_reduce_fusion.3 = (f32[384]{0:T(512)S(1)}, bf16[384,768]{1,0:T(8,128)(2,1)}, bf16[384,768]{1,0:T(8,128)(2,1)}) fusion(f32[384,768]{1,0:T(8,128)S(1)} %fusion.6, f32[384,768]{1,0:T(8,128)S(1)} %fusion.2, f32[384]{0:T(512)S(1)} %mul.81, bf16[384,2048]{1,0:T(8,128)(2,1)S(1)} %bitcast.66, bf16[1,768,2048]{2,1,0:T(8,128)(2,1)S(1)} %copy-done.6), kind=kOutput, calls=%fused_computation.20 | convolution fusion | flops 1212972672 | bytes 8260608 | tf_op jit(solution)/shard_map/dot_general | solution.py:22
  53.8 3.6 %multiply_reduce_fusion = (f32[768]{0:T(1024)S(1)}, bf16[1,768,2048]{2,1,0:T(8,128)(2,1)}) fusion(bf16[384,2048]{1,0:T(8,128)(2,1)S(1)} %bitcast.67, f32[384]{0:T(512)S(1)} %mul.81, f32[384,768]{1,0:T(8,128)S(1)} %fusion.6, f32[384,768]{1,0:T(8,128)S(1)} %fusion.2), kind=kOutput, calls=%fused_computation | convolution fusion | flops 1214741760 | bytes 7082496 | tf_op jit(solution)/shard_map/dot_general | solution.py:16
  58.8 2.6 %fusion = f32[384,2048]{1,0:T(8,128)S(1)} fusion(bf16[384,768]{1,0:T(8,128)(2,1)} %get-tuple-element.66, bf16[1,2048,768]{2,1,0:T(8,128)(2,1)S(1)} %copy-done), kind=kOutput, calls=%fused_computation.3 | convolution fusion | flops 1207959552 | bytes 6881280 | tf_op jit(solution)/shard_map/dot_general | solution.py:22
  61.4 2.6 %add_convert_fusion = bf16[384,2048]{1,0:T(8,128)(2,1)} fusion(f32[384,2048]{1,0:T(8,128)S(1)} %fusion, bf16[384,768]{1,0:T(8,128)(2,1)S(1)} %copy-done.12, bf16[1,2048,768]{2,1,0:T(8,128)(2,1)S(1)} %copy-done.8), kind=kOutput, calls=%fused_computation.16 | convolution fusion | flops 1209532416 | bytes 8454144 | tf_op jit(solution)/shard_map/dot_general | solution.py:22
  64.0 23.5 %return_rows.1 = (bf16[8,48,512]{2,1,0:T(8,128)(2,1)}, f32[8,8,128]{2,1,0:T(8,128)}) custom-call(bf16[8,48,2048]{2,1,0:T(8,128)(2,1)} %bitcast.56, f32[8,8,128]{2,1,0:T(8,128)} %pad.8.gate_ref), custom_call_target="tpu_custom_call" | custom-call | tf_op jit(solution)/shard_map/return_rows/pallas_call | solution.py:409
  87.5 0.8 slice_reduce_fusion.1
  89.5 0.9 fusion.18
  90.4 2.0 %convolution_add_fusion = f32[128,512]{1,0:T(8,128)} fusion(f32[128,512]{1,0:T(8,128)S(1)} %fusion.18, pred[384,128]{1,0:T(8,128)(4,1)S(1)} %fusion.16, bf16[384,512]{1,0:T(8,128)(2,1)} %bitcast.59), kind=kOutput, calls=%fused_computation.25 | convolution fusion | flops 50397184 | bytes 966656 | tf_op jit(solution)/shard_map/dot_general | solution.py:16
  92.4 5.2 %multiply_reduce_fusion.1 = (f32[2048]{0:T(1024)S(1)}, bf16[1,2048,768]{1,2,0:T(8,128)(2,1)}) fusion(bf16[384,2048]{1,0:T(8,128)(2,1)} %bitcast.63, bf16[384,768]{1,0:T(8,128)(2,1)} %get-tuple-element.67), kind=kOutput, calls=%fused_computation.1 | convolution fusion | flops 1212676096 | bytes 5316608 | tf_op jit(solution)/shard_map/dot_general | solution.py:16
  97.6 3.5 %multiply_reduce_fusion.2 = (f32[2048]{0:T(1024)S(1)}, bf16[1,2048,768]{1,2,0:T(8,128)(2,1)}) fusion(bf16[384,2048]{1,0:T(8,128)(2,1)S(1)} %bitcast.65, bf16[384,768]{1,0:T(8,128)(2,1)S(1)} %copy-done.13), kind=kOutput, calls=%fused_computation.2 | convolution fusion | flops 1212676096 | bytes 5316608 | tf_op jit(solution)/shard_map/dot_general | solution.py:16
  101.8 8.8 %small_sums.1 = (f32[2,2048]{1,0:T(2,128)}, f32[1,512]{1,0:T(1,128)}) custom-call(f32[2,2048]{1,0:T(2,128)} %pad_maximum_fusion.square_ref, f32[8,1,512]{2,1,0:T(1,128)} %broadcast_in_dim.63.term_ref), custom_call_target="tpu_custom_call" | custom-call | tf_op jit(solution)/shard_map/small_sums/pallas_call | solution.py:500
  110.6 1.4 %slice_multiply_fusion = (f32[1,2048]{1,0:T(1,128)}, f32[1,2048]{1,0:T(1,128)}) fusion(f32[2,2048]{1,0:T(2,128)} %get-tuple-element.22), kind=kLoop, calls=%fused_computation.38 | loop fusion | flops 4096 | bytes 32768 | tf_op jit(solution)/shard_map/div | solution.py:619
  112.0 4.6 %copy.48 = bf16[1,2048,768]{2,1,0:T(8,128)(2,1)} copy(bf16[1,2048,768]{1,2,0:T(8,128)(2,1)} %get-tuple-element.62) | data formatting | bytes 6291456
  116.7 4.6 %copy.49 = bf16[1,2048,768]{2,1,0:T(8,128)(2,1)} copy(bf16[1,2048,768]{1,2,0:T(8,128)(2,1)} %get-tuple-element.64) | data formatting | bytes 6291456
  (59 shorter events, 6.6 us)
Async XLA Ops:
  0.6 45.0 %copy-start = (bf16[1,2048,768]{2,1,0:T(8,128)(2,1)S(1)}, bf16[1,2048,768]{2,1,0:T(8,128)(2,1)}, u32[]{:S(2)}) copy-start(bf16[1,2048,768]{2,1,0:T(8,128)(2,1)} %param.12) | copy-start | bytes 9437188
  45.6 3.0 %copy-start.7 = (bf16[1,2048,768]{2,1,0:T(8,128)(2,1)S(1)}, bf16[1,2048,768]{2,1,0:T(8,128)(2,1)}, u32[]{:S(2)}) copy-start(bf16[1,2048,768]{2,1,0:T(8,128)(2,1)} %param.13) | copy-start | bytes 9437188
  45.6 3.0 %copy-start.9 = (bf16[8,48,2048]{2,1,0:T(8,128)(2,1)S(1)}, bf16[8,48,2048]{2,1,0:T(8,128)(2,1)}, u32[]{:S(2)}) copy-start(bf16[8,48,2048]{2,1,0:T(8,128)(2,1)} %get-tuple-element.18) | copy-start | bytes 4718596
  48.6 1.9 %copy-start.6 = (bf16[1,768,2048]{2,1,0:T(8,128)(2,1)S(1)}, bf16[1,768,2048]{2,1,0:T(8,128)(2,1)}, u32[]{:S(2)}) copy-start(bf16[1,768,2048]{2,1,0:T(8,128)(2,1)} %param.14) | copy-start | bytes 9437188
  48.6 2.3 %copy-start.11 = (bf16[8,48,2048]{2,1,0:T(8,128)(2,1)S(1)}, bf16[8,48,2048]{2,1,0:T(8,128)(2,1)}, u32[]{:S(2)}) copy-start(bf16[8,48,2048]{2,1,0:T(8,128)(2,1)} %get-tuple-element.17) | copy-start | bytes 4718596
  58.8 2.6 %copy-start.8 = (bf16[1,2048,768]{2,1,0:T(8,128)(2,1)S(1)}, bf16[1,2048,768]{2,1,0:T(8,128)(2,1)}, u32[]{:S(2)}) copy-start(bf16[1,2048,768]{2,1,0:T(8,128)(2,1)} %param.13) | copy-start | bytes 9437188
  58.8 2.6 %copy-start.12 = (bf16[384,768]{1,0:T(8,128)(2,1)S(1)}, bf16[384,768]{1,0:T(8,128)(2,1)}, u32[]{:S(2)}) copy-start(bf16[384,768]{1,0:T(8,128)(2,1)} %get-tuple-element.67) | copy-start | bytes 1769476
  64.0 24.7 %copy-start.4 = (bf16[128,2]{0,1:T(2,128)(2,1)S(1)}, bf16[128,2]{0,1:T(2,128)(2,1)}, u32[]{:S(2)}) copy-start(bf16[128,2]{0,1:T(2,128)(2,1)} %param.10) | copy-start | bytes 1540
  64.0 24.7 %copy-start.3 = (s32[128,2]{0,1:T(2,128)S(1)}, s32[128,2]{0,1:T(2,128)}, u32[]{:S(2)}) copy-start(s32[128,2]{0,1:T(2,128)} %param.9) | copy-start | bytes 3076
  64.0 24.8 %copy-start.1 = (bf16[128,512]{1,0:T(8,128)(2,1)S(1)}, bf16[128,512]{1,0:T(8,128)(2,1)}, u32[]{:S(2)}) copy-start(bf16[128,512]{1,0:T(8,128)(2,1)} %param.8) | copy-start | bytes 393220
  88.7 8.9 %copy-start.2 = (f32[128,2]{0,1:T(2,128)}, f32[128,2]{0,1:T(2,128)S(1)}, u32[]{:S(2)}) copy-start(f32[128,2]{0,1:T(2,128)S(1)} %copy.46) | copy-start | bytes 3076
  92.4 5.2 %copy-start.10 = (bf16[8,48,2048]{2,1,0:T(8,128)(2,1)S(1)}, bf16[8,48,2048]{2,1,0:T(8,128)(2,1)}, u32[]{:S(2)}) copy-start(bf16[8,48,2048]{2,1,0:T(8,128)(2,1)} %get-tuple-element.18) | copy-start | bytes 4718596
  92.4 5.2 %copy-start.13 = (bf16[384,768]{1,0:T(8,128)(2,1)S(1)}, bf16[384,768]{1,0:T(8,128)(2,1)}, u32[]{:S(2)}) copy-start(bf16[384,768]{1,0:T(8,128)(2,1)} %get-tuple-element.66) | copy-start | bytes 1769476
  116.7 4.6 %copy-start.5 = (f32[1,512]{1,0:T(1,128)S(1)}, f32[1,512]{1,0:T(1,128)}, u32[]{:S(2)}) copy-start(f32[1,512]{1,0:T(1,128)} %get-tuple-element.84) | copy-start | bytes 6148

commit v2 on v1

--- a/solution.py
+++ b/solution.py
@@ -37,7 +37,7 @@
     return ep, tp, lax.div(tp, 2), lax.rem(tp, 2)
 
 
-def greet(n_ep, n_tp, all_tp):
+def greet(n_ep, n_tp, all_tp, between=None):
     ep, tp, y, core = place()
     barrier = pltpu.get_barrier_semaphore()
 
@@ -58,25 +58,79 @@
     loop(1, n_ep, to_ep)
     if all_tp:
         loop(1, n_tp, to_tp)
+        if between is not None:
+            between()
         pl.semaphore_wait(barrier, n_ep - 1 + n_tp - 1)
     else:
         loop(1, n_tp // 2, to_y)
         pl.semaphore_signal(
             barrier, inc=1, device_id=(ep, y * 2 + 1 - core), device_id_type=MESH
         )
+        if between is not None:
+            between()
         pl.semaphore_wait(barrier, n_ep - 1 + n_tp // 2)
+
+
+def lane_pick(n_ep, cap, padded):
+    shape = (n_ep, cap, padded)
+    pick = lax.broadcasted_iota(jnp.int32, shape, 1) == lax.broadcasted_iota(jnp.int32, shape, 2)
+    return pick.astype(F32).reshape(n_ep * cap, padded)
+
+
+def own_block(n_ep, cap):
+    shape = (n_ep, n_ep * cap)
+    first = lax.broadcasted_iota(jnp.int32, shape, 0) * cap
+    slot = lax.broadcasted_iota(jnp.int32, shape, 1)
+    return ((slot >= first) & (slot < first + cap)).astype(F32)
+
+
+def fill_slots(routes_ref, weights_ref, tokens_ref, cotangent_ref, table_ref, x_ref, t_ref, w_ref):
+    n_ep, cap, width = x_ref.shape
+    top, tok = routes_ref.shape
+    padded = w_ref.shape[2]
+    routes = routes_ref[...]
+    weights = weights_ref[...].astype(F32)
+    labels = lax.broadcasted_iota(jnp.int32, (n_ep, tok), 0)
+    hit = jnp.zeros((n_ep, tok), F32)
+    chosen = jnp.zeros((n_ep, tok), F32)
+    for k in range(top):
+        same = routes[k : k + 1, :] == labels
+        hit = hit + same.astype(F32)
+        chosen = chosen + jnp.where(same, weights[k : k + 1, :], 0.0)
+    square = (tok, tok)
+    before = lax.broadcasted_iota(jnp.int32, square, 0) < lax.broadcasted_iota(jnp.int32, square, 1)
+    count = jnp.dot(hit.astype(BF16), before.astype(F32).astype(BF16), preferred_element_type=F32)
+    position = jnp.where(hit > 0.0, count, -1.0)
+    slot = lax.broadcasted_iota(jnp.int32, (n_ep, cap, tok), 1).astype(F32)
+    table = (slot == position[:, None, :]).astype(F32).reshape(n_ep * cap, tok).astype(BF16)
+    table_ref[...] = table
+    for source, target in ((tokens_ref, x_ref), (cotangent_ref, t_ref)):
+        rows = jnp.dot(table, source[...], preferred_element_type=F32)
+        target[...] = rows.reshape(n_ep, cap, width).astype(BF16)
+    spread = matmul_nt(chosen.astype(BF16), table) * own_block(n_ep, cap)
+    values = jnp.dot(
+        spread.astype(BF16),
+        lane_pick(n_ep, cap, padded).astype(BF16),
+        preferred_element_type=F32,
+    )
+    w_ref[...] = jnp.broadcast_to(values[:, None, :], w_ref.shape)
 
 
 def dispatch_kernel(
     n_ep,
     n_tp,
     chunks,
+    routes_ref,
+    weights_ref,
+    tokens_ref,
+    cotangent_ref,
+    ox_ref,
+    ot_ref,
+    ow_ref,
+    table_ref,
     x_ref,
     t_ref,
     w_ref,
-    ox_ref,
-    ot_ref,
-    ow_ref,
     ep_send,
     ep_recv,
     y_send,
@@ -90,7 +144,18 @@
     width = x_ref.shape[2]
     per = n_ep // chunks
     partner = y * 2 + 1 - core
-    greet(n_ep, n_tp, False)
+    fill = functools.partial(
+        fill_slots,
+        routes_ref,
+        weights_ref,
+        tokens_ref,
+        cotangent_ref,
+        table_ref,
+        x_ref,
+        t_ref,
+        w_ref,
+    )
+    greet(n_ep, n_tp, False, fill)
     sources = (x_ref, t_ref)
     outs = (ox_ref, ot_ref)
 
@@ -206,8 +271,9 @@
     loop(1, n_ep, drain)
 
 
-def dispatch(input_send, tangent_send, weight_send, n_ep, n_tp):
-    _, cap, width = input_send.shape
+def dispatch(routes, weights, tokens, cotangent, n_ep, n_tp, cap):
+    tok, width = tokens.shape
+    padded = -(-cap // 128) * 128
     chunks = n_ep if n_ep <= 8 else next(c for c in range(8, 0, -1) if n_ep % c == 0)
     n_y = n_tp // 2
     dma = pltpu.SemaphoreType.DMA
@@ -216,11 +282,15 @@
         out_shape=(
             jax.ShapeDtypeStruct((n_ep, cap, width * n_tp), BF16),
             jax.ShapeDtypeStruct((n_ep, cap, width * n_tp), BF16),
-            jax.ShapeDtypeStruct(weight_send.shape, F32),
+            jax.ShapeDtypeStruct((n_ep, 8, padded), F32),
+            jax.ShapeDtypeStruct((n_ep * cap, tok), BF16),
         ),
-        in_specs=[pl.BlockSpec(memory_space=pltpu.VMEM)] * 3,
-        out_specs=[pl.BlockSpec(memory_space=pltpu.VMEM)] * 3,
+        in_specs=[pl.BlockSpec(memory_space=pltpu.VMEM)] * 4,
+        out_specs=[pl.BlockSpec(memory_space=pltpu.VMEM)] * 4,
         scratch_shapes=[
+            pltpu.VMEM((n_ep, cap, width), BF16),
+            pltpu.VMEM((n_ep, cap, width), BF16),
+            pltpu.VMEM((n_ep, 8, padded), F32),
             dma((3, n_ep)),
             dma((3, n_ep)),
             dma((2, n_y, chunks)),
@@ -231,7 +301,7 @@
         ],
         compiler_params=pltpu.CompilerParams(collective_id=0, has_side_effects=True),
         name="dispatch",
-    )(input_send, tangent_send, weight_send)
+    )(routes, weights, tokens, cotangent)
 
 
 def return_kernel(
@@ -518,15 +588,99 @@
     )(square, term)
 
 
-def slot_table(routing, experts, capacity):
-    flat_routes = routing.reshape(-1)
-    labels = lax.broadcasted_iota(jnp.int32, (flat_routes.shape[0], experts), 1)
-    hit_mask = (flat_routes[:, None] == labels).astype(jnp.int32)
-    ranking = jnp.cumsum(hit_mask, axis=0) - 1
-    position = jnp.sum(hit_mask * ranking, axis=1)
-    slot_id = flat_routes * capacity + position
-    slot_index = lax.broadcasted_iota(jnp.int32, (experts * capacity, flat_routes.shape[0]), 0)
-    return slot_index == slot_id[None, :]
+def weight_grads_kernel(x_ref, gate_ref, up_ref, gate_out, up_out, square_out):
+    rows = x_ref.shape[1]
+    for row, (grad, out) in enumerate(((gate_ref, gate_out), (up_ref, up_out))):
+        total = matmul_tn(x_ref[...], grad[...])
+        out[0] = total.astype(BF16)
+        square = jnp.sum(total * total, axis=1, keepdims=True)
+        square_out[row : row + 1, :] = jnp.broadcast_to(square, (rows, 128)).T[0:1, :]
+
+
+def weight_grads(full_input, gate_pre_grad, up_pre_grad):
+    slots, features = full_input.shape
+    hidden = gate_pre_grad.shape[1]
+    rows = min(512, features)
+    whole = pl.BlockSpec((slots, hidden), lambda i: (0, 0))
+    grad = pl.BlockSpec((1, rows, hidden), lambda i: (0, i, 0))
+    return pl.pallas_call(
+        weight_grads_kernel,
+        grid=(features // rows,),
+        out_shape=(
+            jax.ShapeDtypeStruct((1, features, hidden), BF16),
+            jax.ShapeDtypeStruct((1, features, hidden), BF16),
+            jax.ShapeDtypeStruct((2, features), F32),
+        ),
+        in_specs=[pl.BlockSpec((slots, rows), lambda i: (0, i)), whole, whole],
+        out_specs=[grad, grad, pl.BlockSpec((2, rows), lambda i: (0, i))],
+        cost_estimate=pl.CostEstimate(
+            flops=4 * slots * features * hidden,
+            bytes_accessed=4 * features * hidden + 2 * slots * features,
+            transcendentals=0,
+        ),
+        name="weight_grads",
+    )(full_input, gate_pre_grad, up_pre_grad)
+
+
+def combine_kernel(
+    table_ref,
+    back_ref,
+    back_gate_ref,
+    routes_ref,
+    weights_ref,
+    tokens_ref,
+    router_ref,
+    token_out,
+    gate_out,
+    term_out,
+):
+    n_ep, cap, width = back_ref.shape
+    top, tok = routes_ref.shape
+    padded = back_gate_ref.shape[2]
+    tp = lax.axis_index("tp")
+    table = table_ref[...]
+    routes = routes_ref[...]
+    weights = weights_ref[...].astype(F32)
+    labels = lax.broadcasted_iota(jnp.int32, (n_ep, tok), 0)
+    exact = dict(precision=lax.Precision.HIGHEST, preferred_element_type=F32)
+    slot_gate = back_gate_ref[:, 0, :]
+    spread = lax.dot_general(
+        slot_gate, lane_pick(n_ep, cap, padded), (((1,), (1,)), ((), ())), **exact
+    )
+    values = jnp.dot(spread * own_block(n_ep, cap), table.astype(F32), **exact)
+    grads = []
+    mixed = jnp.zeros((1, tok), F32)
+    for k in range(top):
+        same = routes[k : k + 1, :] == labels
+        grads.append(jnp.sum(jnp.where(same, values, 0.0), axis=0, keepdims=True))
+        gate_out[k : k + 1, :] = grads[k]
+        mixed = mixed + weights[k : k + 1, :] * grads[k]
+    signal = jnp.zeros((n_ep, tok), F32)
+    for k in range(top):
+        logit = weights[k : k + 1, :] * (grads[k] - mixed)
+        signal = signal + jnp.where(routes[k : k + 1, :] == labels, logit, 0.0)
+    signal = signal.astype(BF16)
+    term = jnp.dot(signal, tokens_ref[...], preferred_element_type=F32)
+    for e in range(n_ep):
+        term_out[e] = term[e : e + 1, :]
+    back = back_ref[...].astype(F32).reshape(n_ep * cap, width).astype(BF16)
+    cols = pl.ds(pl.multiple_of(tp * width, width), width)
+    token_out[...] = matmul_tn(table, back) + matmul_tn(signal, router_ref[:, cols])
+
+
+def combine(table, back_rows, back_gate, routes, weights, tokens, router_rows):
+    experts = router_rows.shape[0]
+    return pl.pallas_call(
+        combine_kernel,
+        out_shape=(
+            jax.ShapeDtypeStruct(tokens.shape, F32),
+            jax.ShapeDtypeStruct(routes.shape, F32),
+            jax.ShapeDtypeStruct((experts, 1, tokens.shape[1]), F32),
+        ),
+        in_specs=[pl.BlockSpec(memory_space=pltpu.VMEM)] * 7,
+        out_specs=[pl.BlockSpec(memory_space=pltpu.VMEM)] * 3,
+        name="combine",
+    )(table, back_rows, back_gate, routes, weights, tokens, router_rows)
 
 
 def lanes(slot_values, experts, capacity):
@@ -544,18 +698,9 @@
     capacity = 3 * top_count * tok_rows // (2 * experts)
     slot_count = experts * capacity
     features = local_width * n_tp
-    matches = slot_table(routing, experts, capacity)
-    by_token = jnp.any(matches.reshape(slot_count, tok_rows, top_count), axis=2).astype(BF16)
-    input_send = jnp.dot(by_token, tokens, preferred_element_type=F32).astype(BF16)
-    tangent_send = jnp.dot(by_token, cotangent, preferred_element_type=F32).astype(BF16)
-    weight_flat = gate_weights.reshape(-1).astype(F32)
-    weight_send = jnp.sum(jnp.where(matches, weight_flat[None, :], 0.0), axis=1)
-    full_input, full_tangent, weight_slots = dispatch(
-        input_send.reshape(experts, capacity, local_width),
-        tangent_send.reshape(experts, capacity, local_width),
-        lanes(weight_send, experts, capacity),
-        n_ep,
-        n_tp,
+    routes, weights = routing.T, gate_weights.T
+    full_input, full_tangent, weight_slots, table = dispatch(
+        routes, weights, tokens, cotangent, n_ep, n_tp, capacity
     )
     full_input = full_input.reshape(slot_count, features)
     full_tangent = full_tangent.reshape(slot_count, features)
@@ -577,8 +722,7 @@
         hidden_grad * pre_up * sigmoid_gate * (1.0 + pre_gate * (1.0 - sigmoid_gate))
     ).astype(BF16)
     up_pre_grad = (hidden_grad * active).astype(BF16)
-    gate_sum = matmul_tn(full_input, gate_pre_grad)
-    up_sum = matmul_tn(full_input, up_pre_grad)
+    gate_proj_grad, up_proj_grad, squares = weight_grads(full_input, gate_pre_grad, up_pre_grad)
     down_sum = matmul_tn(scaled, full_tangent)
     unit_count = hidden_local * n_tp
     slot_grad = (
@@ -590,29 +734,15 @@
         n_ep,
         n_tp,
     )
-    back_flat = back_rows.reshape(slot_count, local_width)
-    token_part = matmul_tn(by_token, back_flat)
-    gate_slots = back_gate[:, 0, :capacity].reshape(slot_count, 1)
-    gate_grad = jnp.sum(jnp.where(matches, gate_slots, 0.0), axis=0).reshape(tok_rows, top_count)
-    weights_f = gate_weights.astype(F32)
-    mixed_term = jnp.sum(weights_f * gate_grad, axis=1, keepdims=True)
-    logit_grad = weights_f * (gate_grad - mixed_term)
-    labels = lax.broadcasted_iota(jnp.int32, (1, 1, experts), 2)
-    signal = jnp.sum(
-        jnp.where(routing[:, :, None] == labels, logit_grad[:, :, None], 0.0), axis=1
-    ).astype(BF16)
-    router_term = matmul_tn(signal, tokens)
-    squares = jnp.stack([jnp.sum(gate_sum * gate_sum, axis=1), jnp.sum(up_sum * up_sum, axis=1)])
-    squares, router_grad = small_sums(squares, router_term[:, None, :], n_ep, n_tp)
-    router_cols = lax.dynamic_slice_in_dim(
-        router, lax.axis_index("tp") * local_width, local_width, 0
-    )
-    token_grad = token_part + matmul_nt(signal, router_cols)
+    token_grad, gate_grad, router_term = combine(
+        table, back_rows, back_gate, routes, weights, tokens, router.T
+    )
+    squares, router_grad = small_sums(squares, router_term, n_ep, n_tp)
     return (
         token_grad,
-        gate_grad,
-        gate_sum.astype(BF16)[None],
-        up_sum.astype(BF16)[None],
+        gate_grad.T,
+        gate_proj_grad,
+        up_proj_grad,
         down_sum.astype(BF16)[None],
         router_grad,
         squares[0:1] / unit_count,

time: 123 us -> 101 us (0.82)
  matrix products: 31.6 us -> 16 us
  local copies, waits for them, and re-layouts: 17.9 us -> 4.38 us
  Pallas kernels: 67.7 us -> 77.4 us
  other arithmetic: 3.86 us -> 1.42 us
    dot_general x5 -> x1, matrix products: 14.5 us -> 3.64 us  [matmul_tn(): lax.dot_general(left_side, right_side, (((0,), (0,)), ((), ())), preferre...]
    pallas_call x0 -> x2, Pallas kernels: none -> 9.68 us  [the longest x1 6.9 us: weight_grads(): pl.pallas_call(weight_grads_kernel, grid=(features // rows,), out_shape=(...]
    unnamed x32 -> x15, local copies, waits for them, and re-layouts: 11.8 us -> 2.23 us
    dot_general x2 -> x0, matrix products: 3.8 us -> none  [the longest x1 1.9 us: shards(): jnp.dot(by_token, cotangent, preferred_element_type=F32).astype(BF16)]
    another operation x3 -> x0, other arithmetic: 1.25 us -> none
    dot_general x4 -> x3, matrix products: 8.97 us -> 8.06 us  [matmul_nt(): lax.dot_general(left_side, right_side, (((1,), (1,)), ((), ())), preferre...]
where the time goes in v2:
time: 101 us; the launch traced here: 100 us
  Pallas kernels  77.4 us (77%)
  matrix products  16 us (16%)
  local copies, waits for them, and re-layouts  4.38 us (4%)
  other arithmetic  1.42 us (1%)
    pallas_call x1, Pallas kernels, dispatch(): pl.pallas_call(functools.partial(dispatch_kernel, n_ep, n_tp, chunks), ou...  35.4 us
    pallas_call x1, Pallas kernels, return_rows(): pl.pallas_call(functools.partial(return_kernel, n_ep, n_tp, chunks), out_...  23.4 us
    pallas_call x1, Pallas kernels, small_sums(): pl.pallas_call(functools.partial(sums_kernel, n_ep, n_tp), out_shape=(jax...  8.83 us
    dot_general x3, matrix products, matmul_nt(): lax.dot_general(left_side, right_side, (((1,), (1,)), ((), ())), preferre...  8.06 us
    pallas_call x1, Pallas kernels, weight_grads(): pl.pallas_call(weight_grads_kernel, grid=(features // rows,), out_shape=(...  6.9 us
    dot_general x1, matrix products, matmul_tn(): lax.dot_general(left_side, right_side, (((0,), (0,)), ((), ())), preferre...  3.64 us
    dot_general x1, matrix products, shards(): pre_gate = jnp.dot(full_input, gate_matrix, preferred_element_type=F32)  2.93 us
    pallas_call x1, Pallas kernels, combine(): pl.pallas_call(combine_kernel, out_shape=(jax.ShapeDtypeStruct(tokens.sha...  2.78 us

profile of v2, /device:TPU:0, one launch (start us, length us, event | category | flops | bytes accessed | tf_op | source)
XLA Modules:
  0.0 100.0 jit_solution(15567720080325406733)
XLA Ops:
  0.6 0.0 copy-start
  0.7 35.4 %dispatch.1 = (bf16[8,48,2048]{2,1,0:T(8,128)(2,1)}, bf16[8,48,2048]{2,1,0:T(8,128)(2,1)}, f32[8,8,128]{2,1,0:T(8,128)}, bf16[384,128]{1,0:T(8,128)(2,1)}) custom-call(s32[2,128]{1,0:T(2,128)} %bitcast.34, bf16[2,128]{1,0:T(2,128)(2,1)} %bitcast.36, bf16[128,512]{1,0:T(8,128)(2,1)} %tokens_ref.3, bf16[128,512]{1,0:T(8,128)(2,1)} %cotangent_ref.1), custom_call_target="tpu_custom_call" | custom-call | tf_op jit(solution)/shard_map/dispatch/pallas_call | solution.py:280
  36.1 0.8 slice_reduce_fusion
  36.9 0.1 mul.43
  37.0 0.0 copy-start.2
  37.0 0.0 copy-start.4
  37.0 2.9 %fusion.2 = f32[384,768]{1,0:T(8,128)S(1)} fusion(bf16[384,2048]{1,0:T(8,128)(2,1)} %bitcast.38, bf16[1,2048,768]{2,1,0:T(8,128)(2,1)S(1)} %copy-done), kind=kOutput, calls=%fused_computation.3 | convolution fusion | flops 1207959552 | bytes 5898240 | tf_op jit(solution)/shard_map/dot_general | solution.py:712
  39.9 0.0 copy-start.1
  40.0 1.4 %fusion.6 = f32[384,768]{1,0:T(8,128)S(1)} fusion(bf16[384,2048]{1,0:T(8,128)(2,1)S(1)} %bitcast.40, bf16[1,2048,768]{2,1,0:T(8,128)(2,1)S(1)} %copy-done.2), kind=kOutput, calls=%fused_computation.7 | convolution fusion | flops 1207959552 | bytes 5898240 | tf_op jit(solution)/shard_map/dot_general | solution.py:713
  41.4 0.5 copy-done.1
  41.8 0.5 copy-done.5
  42.3 2.9 %multiply_reduce_fusion.1 = (f32[384]{0:T(512)S(1)}, bf16[384,768]{1,0:T(8,128)(2,1)}, bf16[384,768]{1,0:T(8,128)(2,1)}) fusion(f32[384,768]{1,0:T(8,128)S(1)} %fusion.6, f32[384,768]{1,0:T(8,128)S(1)} %fusion.2, f32[384]{0:T(512)S(1)} %mul.43, bf16[384,2048]{1,0:T(8,128)(2,1)S(1)} %bitcast.41, bf16[1,768,2048]{2,1,0:T(8,128)(2,1)S(1)} %copy-done.1), kind=kOutput, calls=%fused_computation.14 | convolution fusion | flops 1212972672 | bytes 8260608 | tf_op jit(solution)/shard_map/dot_general | solution.py:22
  45.2 3.6 %multiply_reduce_fusion = (f32[768]{0:T(1024)S(1)}, bf16[1,768,2048]{2,1,0:T(8,128)(2,1)}) fusion(bf16[384,2048]{1,0:T(8,128)(2,1)S(1)} %bitcast.42, f32[384]{0:T(512)S(1)} %mul.43, f32[384,768]{1,0:T(8,128)S(1)} %fusion.6, f32[384,768]{1,0:T(8,128)S(1)} %fusion.2), kind=kOutput, calls=%fused_computation | convolution fusion | flops 1214741760 | bytes 7082496 | tf_op jit(solution)/shard_map/dot_general | solution.py:16
  48.8 0.6 div.22
  49.4 0.1 reshape.43
  49.5 0.6 pad.4.gate_ref
  50.1 2.6 %fusion = f32[384,2048]{1,0:T(8,128)S(1)} fusion(bf16[384,768]{1,0:T(8,128)(2,1)} %get-tuple-element.40.gate_ref, bf16[1,2048,768]{2,1,0:T(8,128)(2,1)S(1)} %copy-done), kind=kOutput, calls=%fused_computation.1 | convolution fusion | flops 1207959552 | bytes 6881280 | tf_op jit(solution)/shard_map/dot_general | solution.py:22
  52.8 2.6 %add_convert_fusion = bf16[384,2048]{1,0:T(8,128)(2,1)} fusion(f32[384,2048]{1,0:T(8,128)S(1)} %fusion, bf16[384,768]{1,0:T(8,128)(2,1)S(1)} %copy-done.6, bf16[1,2048,768]{2,1,0:T(8,128)(2,1)S(1)} %copy-done.3), kind=kOutput, calls=%fused_computation.12 | convolution fusion | flops 1209532416 | bytes 8454144 | tf_op jit(solution)/shard_map/dot_general | solution.py:22
  55.3 23.4 %return_rows.1 = (bf16[8,48,512]{2,1,0:T(8,128)(2,1)}, f32[8,8,128]{2,1,0:T(8,128)}) custom-call(bf16[8,48,2048]{2,1,0:T(8,128)(2,1)} %bitcast.32, f32[8,8,128]{2,1,0:T(8,128)} %pad.4.gate_ref), custom_call_target="tpu_custom_call" | custom-call | tf_op jit(solution)/shard_map/return_rows/pallas_call | solution.py:479
  78.8 2.8 %combine.1 = (f32[128,512]{1,0:T(8,128)}, f32[2,128]{1,0:T(2,128)}, f32[8,1,512]{2,1,0:T(1,128)}) custom-call(bf16[384,128]{1,0:T(8,128)(2,1)} %get-tuple-element.23.table_ref, bf16[8,48,512]{2,1,0:T(8,128)(2,1)} %get-tuple-element.27.back_ref, f32[8,8,128]{2,1,0:T(8,128)} %get-tuple-element.28.back_gate_ref, s32[2,128]{1,0:T(2,128)} %bitcast.35, ...), custom_call_target="tpu_custom_call" | custom-call | tf_op jit(solution)/shard_map/combine/pallas_call | solution.py:673
  81.5 6.9 %weight_grads.1 = (bf16[1,2048,768]{2,1,0:T(8,128)(2,1)}, bf16[1,2048,768]{2,1,0:T(8,128)(2,1)}, f32[2,2048]{1,0:T(2,128)}) custom-call(bf16[384,2048]{1,0:T(8,128)(2,1)} %bitcast.39, bf16[384,768]{1,0:T(8,128)(2,1)} %get-tuple-element.40.gate_ref, bf16[384,768]{1,0:T(8,128)(2,1)} %get-tuple-element.41.up_ref), custom_call_target="tpu_custom_call" | custom-call | flops 2415919104 | bytes 7864320 | tf_op jit(solution)/shard_map/weight_grads/pallas_call | solution.py:606
  88.4 8.8 %small_sums.1 = (f32[2,2048]{1,0:T(2,128)}, f32[1,512]{1,0:T(1,128)}) custom-call(f32[2,2048]{1,0:T(2,128)} %get-tuple-element.33.square_ref, f32[8,1,512]{2,1,0:T(1,128)} %get-tuple-element.34.term_ref), custom_call_target="tpu_custom_call" | custom-call | tf_op jit(solution)/shard_map/small_sums/pallas_call | solution.py:570
  97.3 1.4 %slice_multiply_fusion = (f32[1,2048]{1,0:T(1,128)}, f32[1,2048]{1,0:T(1,128)}) fusion(f32[2,2048]{1,0:T(2,128)} %get-tuple-element.36), kind=kLoop, calls=%fused_computation.22 | loop fusion | flops 4096 | bytes 32768 | tf_op jit(solution)/shard_map/div | solution.py:749
  98.7 1.3 %copy.18 = f32[1,512]{1,0:T(1,128)} copy(f32[1,512]{1,0:T(1,128)} %get-tuple-element.58) | data formatting | bytes 4096
  (9 shorter events, 0.0 us)
Async XLA Ops:
  0.6 36.3 %copy-start = (bf16[1,2048,768]{2,1,0:T(8,128)(2,1)S(1)}, bf16[1,2048,768]{2,1,0:T(8,128)(2,1)}, u32[]{:S(2)}) copy-start(bf16[1,2048,768]{2,1,0:T(8,128)(2,1)} %param.12) | copy-start | bytes 9437188
  37.0 3.0 %copy-start.2 = (bf16[1,2048,768]{2,1,0:T(8,128)(2,1)S(1)}, bf16[1,2048,768]{2,1,0:T(8,128)(2,1)}, u32[]{:S(2)}) copy-start(bf16[1,2048,768]{2,1,0:T(8,128)(2,1)} %param.13) | copy-start | bytes 9437188
  37.0 3.0 %copy-start.4 = (bf16[8,48,2048]{2,1,0:T(8,128)(2,1)S(1)}, bf16[8,48,2048]{2,1,0:T(8,128)(2,1)}, u32[]{:S(2)}) copy-start(bf16[8,48,2048]{2,1,0:T(8,128)(2,1)} %get-tuple-element.26) | copy-start | bytes 4718596
  39.9 1.9 %copy-start.1 = (bf16[1,768,2048]{2,1,0:T(8,128)(2,1)S(1)}, bf16[1,768,2048]{2,1,0:T(8,128)(2,1)}, u32[]{:S(2)}) copy-start(bf16[1,768,2048]{2,1,0:T(8,128)(2,1)} %param.14) | copy-start | bytes 9437188
  39.9 2.3 %copy-start.5 = (bf16[8,48,2048]{2,1,0:T(8,128)(2,1)S(1)}, bf16[8,48,2048]{2,1,0:T(8,128)(2,1)}, u32[]{:S(2)}) copy-start(bf16[8,48,2048]{2,1,0:T(8,128)(2,1)} %get-tuple-element.25) | copy-start | bytes 4718596
  50.1 2.6 %copy-start.3 = (bf16[1,2048,768]{2,1,0:T(8,128)(2,1)S(1)}, bf16[1,2048,768]{2,1,0:T(8,128)(2,1)}, u32[]{:S(2)}) copy-start(bf16[1,2048,768]{2,1,0:T(8,128)(2,1)} %param.13) | copy-start | bytes 9437188
  50.1 2.6 %copy-start.6 = (bf16[384,768]{1,0:T(8,128)(2,1)S(1)}, bf16[384,768]{1,0:T(8,128)(2,1)}, u32[]{:S(2)}) copy-start(bf16[384,768]{1,0:T(8,128)(2,1)} %get-tuple-element.41.up_ref) | copy-start | bytes 1769476
